TPU v7x, 32 devices: a whole 2x2x4 slice. The times are simulated.
32 devices in a mesh: sp: 16 (over z, y, x), tp: 2 (over core).
Axes of the slice: x: 2, y: 2, z: 4, core: 2. Of those that a mesh axis runs over, the one named last changes fastest.
Arguments:
- tokens: bfloat16 [4096, 3072], P('sp', 'tp'), may hold values from -6 to 6
- norm_gain: float32 [3072], replicated, may hold values from 0.1 to 1.9
- outer_gate_w: bfloat16 [3072, 1536], P('sp', 'tp'), may hold values from -0.109375 to 0.109375
- inner_gate_w: bfloat16 [3072, 1536], P('sp', 'tp'), may hold values from -0.109375 to 0.109375
- signal_w: bfloat16 [3072, 1536], P('sp', 'tp'), may hold values from -0.109375 to 0.109375
- conv_taps: float32 [3, 1536], P(None, 'tp'), may hold values from -3.5 to 3.5
- query_w: bfloat16 [3072, 1536], P('sp', 'tp'), may hold values from -1.5 to 1.5
- key_w: bfloat16 [3072, 512], P('sp', 'tp'), may hold values from -1.5 to 1.5
- value_w: bfloat16 [3072, 512], P('sp', 'tp'), may hold values from -0.109375 to 0.109375
- sink_logits: float32 [24], P('tp'), may hold values from -1 to 5
- out_conv_w: bfloat16 [1536, 3072], P('tp', 'sp'), may hold values from -0.109375 to 0.109375
- out_attn_w: bfloat16 [1536, 3072], P('tp', 'sp'), may hold values from -0.109375 to 0.109375
Outputs:
- mixed: bfloat16 [4096, 3072], P(('sp', 'tp'))
All inputs are finite; a program needn't handle non-finite values.
Results may differ from a plain program's by a relative error of at most 0.02.
Values may be sent and summed in bfloat16 or wider, within the bound.
A program may use at most 64 MiB of HBM per device.

v0:
```python
import jax
import jax.numpy as jnp
from jax import lax
from jax.sharding import PartitionSpec as P

QHEADS = 24
KVHEADS = 8
HEAD = 64
TAPS = 3
WINDOW = 128


def from_behind(value, axis, steps):
    count = lax.axis_size(axis)
    initial, last = (max(0, -steps), min(count, count - steps))
    return lax.ppermute(value, axis, [(source, source + steps) for source in range(initial, last)])


def add_products(pieces, normed):
    return tuple((jnp.dot(normed, piece, preferred_element_type=jnp.float32) for piece in pieces))


def convolve(gated, before, outer, conv_taps):
    extended = jnp.concatenate([before, gated], axis=0).astype(jnp.float32)
    length = gated.shape[0]
    conv = sum((conv_taps[k] * extended[k : k + length] for k in range(conv_taps.shape[0])))
    return (outer.astype(jnp.float32) * conv).astype(jnp.bfloat16)


def attention(queries, keys_ext, values_ext, sink_logits, offset):
    f32 = jnp.float32
    length = queries.shape[0]
    kv_local = keys_ext.shape[1] // HEAD
    group = QHEADS // KVHEADS
    heads_local = kv_local * group
    span = min(512, length)
    first = lax.axis_index("tp") * heads_local + 1
    slopes = jnp.exp2(
        -8.0 * (first + jnp.arange(heads_local, dtype=jnp.int32)).astype(f32) / QHEADS
    ).reshape(kv_local, group)
    sinks = sink_logits.reshape(kv_local, group)[:, :, None]

    def attend(block):
        start = block * span
        qblock = queries.reshape(span, kv_local, group, HEAD)
        kblock = keys_ext.reshape(span + WINDOW, kv_local, HEAD)
        vblock = values_ext.reshape(span + WINDOW, kv_local, HEAD)
        scores = jnp.einsum(
            "qhgd,shd->hgqs", qblock, kblock, preferred_element_type=f32
        ) * HEAD ** (-0.5)
        qpos = offset + start + jnp.arange(span, dtype=jnp.int32)
        kpos = offset + start - WINDOW + jnp.arange(span + WINDOW, dtype=jnp.int32)
        dist = qpos[:, None] - kpos[None, :]
        valid = (dist >= 0) & (dist < WINDOW) & (kpos >= 0)[None, :]
        scores = scores - slopes[:, :, None, None] * dist.astype(f32)
        scores = jnp.where(valid, scores, -1e30)
        top = jnp.maximum(jnp.max(scores, axis=-1), sinks)
        expo = jnp.exp(scores - top[..., None])
        total = jnp.sum(expo, axis=-1) + jnp.exp(sinks - top)
        probs = (expo / total[..., None]).astype(jnp.bfloat16)
        out = jnp.einsum("hgqs,shd->qhgd", probs, vblock, preferred_element_type=f32)
        return out.reshape(span, heads_local * HEAD)

    blocks = lax.map(attend, jnp.arange(length // span, dtype=jnp.int32))
    return blocks.reshape(length, heads_local * HEAD).astype(jnp.bfloat16)


def body(
    tokens,
    norm_gain,
    outer_gate_w,
    inner_gate_w,
    signal_w,
    conv_taps,
    query_w,
    key_w,
    value_w,
    sink_logits,
    out_conv_w,
    out_attn_w,
):
    f32 = jnp.float32
    bf16 = jnp.bfloat16
    whole = lax.all_gather(tokens, "tp", axis=1, tiled=True)
    x32 = whole.astype(f32)
    normed = (
        x32 * lax.rsqrt(jnp.mean(x32 * x32, axis=-1, keepdims=True) + 1e-06) * norm_gain
    ).astype(bf16)
    length = normed.shape[0]
    offset = lax.axis_index("sp") * length

    def fold_rows(pieces):
        return add_products(pieces, normed)

    conv_weights = (outer_gate_w, inner_gate_w, signal_w)
    conv_results = fold_rows(
        (
            lax.all_gather(conv_weights[0], "sp", axis=0, tiled=True),
            lax.all_gather(conv_weights[1], "sp", axis=0, tiled=True),
            lax.all_gather(conv_weights[2], "sp", axis=0, tiled=True),
        )
    )
    outer, inner, signal = tuple((result.astype(bf16) for result in conv_results))
    gated = (inner.astype(f32) * signal.astype(f32)).astype(bf16)
    before = from_behind(gated[length - TAPS + 1 :], "sp", 1)
    conv_out = convolve(gated, before, outer, conv_taps)
    attn_weights = (query_w, key_w, value_w)
    attn_results = fold_rows(
        (
            lax.all_gather(attn_weights[0], "sp", axis=0, tiled=True),
            lax.all_gather(attn_weights[1], "sp", axis=0, tiled=True),
            lax.all_gather(attn_weights[2], "sp", axis=0, tiled=True),
        )
    )
    queries, keys, values = tuple((result.astype(bf16) for result in attn_results))
    keys_before, values_before = from_behind(
        (keys[length - WINDOW :], values[length - WINDOW :]), "sp", 1
    )
    keys_ext = jnp.concatenate([keys_before, keys], axis=0)
    values_ext = jnp.concatenate([values_before, values], axis=0)
    attn_out = attention(queries, keys_ext, values_ext, sink_logits, offset)
    conv_whole, attn_whole = (
        lax.all_gather(out_conv_w, "sp", axis=1, tiled=True),
        lax.all_gather(out_attn_w, "sp", axis=1, tiled=True),
    )
    result = jnp.dot(conv_out, conv_whole, preferred_element_type=f32)
    mixed = lax.psum_scatter(
        (result + jnp.dot(attn_out, attn_whole, preferred_element_type=f32)).astype(jnp.bfloat16),
        "tp",
        scatter_dimension=0,
        tiled=True,
    ).astype(jnp.float32)
    return mixed.astype(bf16)


def solution(mesh):
    in_specs = (
        P("sp", "tp"),
        P(),
        P("sp", "tp"),
        P("sp", "tp"),
        P("sp", "tp"),
        P(None, "tp"),
        P("sp", "tp"),
        P("sp", "tp"),
        P("sp", "tp"),
        P("tp"),
        P("tp", "sp"),
        P("tp", "sp"),
    )
    out_specs = P(("sp", "tp"), None)
    return jax.shard_map(body, mesh=mesh, in_specs=in_specs, out_specs=out_specs, check_vma=False)
```

profile of v0, /device:TPU:1, one launch (start us, length us, event | category | flops | bytes accessed | tf_op | source)
XLA Modules:
  0.0 649.1 jit_solution(15661393030916549950)
XLA Ops:
  6.5 0.7 all-gather.10.cloned.1.call-update
  7.3 0.7 all-gather.22.cloned.1.call-update
  10.5 0.7 all-gather.12.cloned.1.call-update
  11.3 0.7 all-gather.18.cloned.1.call-update
  12.8 0.7 max.21
  13.5 0.8 slice_reduce_fusion.2
  14.7 6.5 all-gather.10.cloned.1.call-done
  21.2 1.9 fusion.3
  23.1 57.9 %all-gather.22.cloned.1.call-done = bf16[3072,256]{1,0:T(8,128)(2,1)} async-done(((bf16[192,256]{1,0:T(8,128)(2,1)}), bf16[3072,256]{1,0:T(8,128)(2,1)}) %all-gather.22.cloned.1.call-update) | async-done | bytes 1572880 | tf_op jit(solution)/shard_map/all_gather | solution.py:111
  81.0 2.5 convolution_convert_fusion.4
  83.5 3.1 collective-permute-start.2
  86.6 53.9 %all-gather.20.cloned.1.call-done = bf16[3072,256]{1,0:T(8,128)(2,1)} async-done(((bf16[192,256]{1,0:T(8,128)(2,1)}), bf16[3072,256]{1,0:T(8,128)(2,1)}) %all-gather.20.cloned.1.call-update) | async-done | bytes 1572880 | tf_op jit(solution)/shard_map/all_gather | solution.py:112
  140.5 2.0 convolution_convert_fusion.5
  142.6 3.1 collective-permute-start.1
  145.8 1.1 collective-permute-done.1
  147.1 74.4 %all-gather.24.cloned.1.call-done = bf16[3072,768]{1,0:T(8,128)(2,1)} async-done(((bf16[192,768]{1,0:T(8,128)(2,1)}), bf16[3072,768]{1,0:T(8,128)(2,1)}) %all-gather.24.cloned.1.call-update) | async-done | bytes 4718608 | tf_op jit(solution)/shard_map/all_gather | solution.py:110
  221.5 3.8 convolution_convert_fusion
  225.5 77.1 %all-gather.14.cloned.1.call-done = bf16[3072,768]{1,0:T(8,128)(2,1)} async-done(((bf16[192,768]{1,0:T(8,128)(2,1)}), bf16[3072,768]{1,0:T(8,128)(2,1)}) %all-gather.14.cloned.1.call-update) | async-done | bytes 4718608 | tf_op jit(solution)/shard_map/all_gather | solution.py:99
  302.5 4.7 fusion.11
  307.2 76.4 %all-gather.16.cloned.1.call-done = bf16[3072,768]{1,0:T(8,128)(2,1)} async-done(((bf16[192,768]{1,0:T(8,128)(2,1)}), bf16[3072,768]{1,0:T(8,128)(2,1)}) %all-gather.16.cloned.1.call-update) | async-done | bytes 4718608 | tf_op jit(solution)/shard_map/all_gather | solution.py:100
  383.6 4.0 fusion.10
  387.6 3.3 collective-permute-start
  390.8 1.3 fusion.6
  392.2 1.3 fusion.1
  393.6 1.7 fusion.15
  395.4 1.0 maximum_convert_fusion
  396.4 68.4 %all-gather.12.cloned.1.call-done = bf16[3072,768]{1,0:T(8,128)(2,1)} async-done(((bf16[192,768]{1,0:T(8,128)(2,1)}), bf16[3072,768]{1,0:T(8,128)(2,1)}) %all-gather.12.cloned.1.call-update) | async-done | bytes 4718608 | tf_op jit(solution)/shard_map/all_gather | solution.py:98
  464.8 81.2 %all-gather.18.cloned.1.call-done = bf16[768,3072]{0,1:T(8,128)(2,1)} async-done(((bf16[768,192]{0,1:T(8,128)(2,1)}), bf16[768,3072]{0,1:T(8,128)(2,1)}) %all-gather.18.cloned.1.call-update) | async-done | bytes 4718608 | tf_op jit(solution)/shard_map/all_gather | solution.py:123
  545.9 8.3 %fusion.18 = f32[256,3072]{1,0:T(8,128)S(1)} fusion(bf16[768,3072]{0,1:T(8,128)(2,1)} %all-gather.18.cloned.1.call-done, bf16[3072,768]{1,0:T(8,128)(2,1)} %all-gather.12.cloned.1.call-done, f32[258,768]{1,0:T(8,128)} %maximum_convert_fusion, f32[768]{0:T(1024)S(1)} %get-tuple-element.20, f32[768]{0:T(1024)S(1)} %get-tuple-element.21, ...), kind=kOutput, calls=%fused_computation.36 | convolution fusion | flops 2420834304 | bytes 16537600 | tf_op jit(solution)/shard_map/dot_general | solution.py:126
  554.3 72.8 %all-gather.26.cloned.1.call-done = bf16[768,3072]{0,1:T(8,128)(2,1)} async-done(((bf16[768,192]{0,1:T(8,128)(2,1)}), bf16[768,3072]{0,1:T(8,128)(2,1)}) %all-gather.26.cloned.1.call-update) | async-done | bytes 4718608 | tf_op jit(solution)/shard_map/all_gather | solution.py:124
  627.1 5.0 fusion.2
  632.1 10.1 %reduce-scatter.2.cloned.1.call-done = bf16[128,3072]{1,0:T(8,128)(2,1)} async-done(((bf16[256,3072]{1,0:T(8,128)(2,1)}), bf16[128,3072]{1,0:T(8,128)(2,1)}) %reduce-scatter.2.cloned.1.call-update) | async-done | bytes 786448 | tf_op jit(solution)/shard_map/reduce_scatter | solution.py:127
  (41 shorter events, 4.3 us)
Async XLA Ops:
  6.5 74.5 %copy-start.2 = (f32[3072]{0:T(1024)S(1)}, f32[3072]{0:T(1024)}, u32[]{:S(2)}) copy-start(f32[3072]{0:T(1024)} %param.13) | copy-start | bytes 36868
  6.5 14.6 %all-gather.10.cloned.1.call-start = ((), (), s32[]{:S(2)}) async-start(), calls=%async_computation.1 | async-start | bytes 2359296 | tf_op jit(solution)/shard_map/all_gather | solution.py:84
  7.3 73.8 %all-gather.22.cloned.1.call-start = ((), (), s32[]{:S(2)}) async-start(), calls=%async_computation.7 | async-start | bytes 1671168 | tf_op jit(solution)/shard_map/all_gather | solution.py:111
  8.0 132.5 %all-gather.20.cloned.1.call-start = ((), (), s32[]{:S(2)}) async-start(), calls=%async_computation.6 | async-start | bytes 1671168 | tf_op jit(solution)/shard_map/all_gather | solution.py:112
  8.7 212.8 %all-gather.24.cloned.1.call-start = ((), (), s32[]{:S(2)}) async-start(), calls=%async_computation.8 | async-start | bytes 5013504 | tf_op jit(solution)/shard_map/all_gather | solution.py:110
  9.3 293.2 %all-gather.14.cloned.1.call-start = ((), (), s32[]{:S(2)}) async-start(), calls=%async_computation.3 | async-start | bytes 5013504 | tf_op jit(solution)/shard_map/all_gather | solution.py:99
  9.9 373.7 %all-gather.16.cloned.1.call-start = ((), (), s32[]{:S(2)}) async-start(), calls=%async_computation.4 | async-start | bytes 5013504 | tf_op jit(solution)/shard_map/all_gather | solution.py:100
  10.5 454.3 %all-gather.12.cloned.1.call-start = ((), (), s32[]{:S(2)}) async-start(), calls=%async_computation.2 | async-start | bytes 5013504 | tf_op jit(solution)/shard_map/all_gather | solution.py:98
  11.2 534.7 %all-gather.18.cloned.1.call-start = ((), (), s32[]{:S(2)}) async-start(), calls=%async_computation.5 | async-start | bytes 5013504 | tf_op jit(solution)/shard_map/all_gather | solution.py:123
  12.0 615.1 %all-gather.26.cloned.1.call-start = ((), (), s32[]{:S(2)}) async-start(), calls=%async_computation.9 | async-start | bytes 5013504 | tf_op jit(solution)/shard_map/all_gather | solution.py:124
  12.7 629.5 %reduce-scatter.2.cloned.1.call-start = ((), (), s32[]{:S(2)}) async-start(), calls=%async_computation.10 | async-start | bytes 2359296 | tf_op jit(solution)/shard_map/reduce_scatter | solution.py:127
  21.2 119.3 %copy-start = (bf16[256,3072]{1,0:T(8,128)(2,1)S(1)}, bf16[256,3072]{1,0:T(8,128)(2,1)}, u32[]{:S(2)}) copy-start(bf16[256,3072]{1,0:T(8,128)(2,1)} %all-gather.10.cloned.1.call-done) | copy-start | bytes 4718596
  23.1 360.5 %copy-start.1 = (f32[256]{0:T(256)}, f32[256]{0:T(256)S(1)}, u32[]{:S(2)}) copy-start(f32[256]{0:T(256)S(1)} %add_rsqrt_fusion) | copy-start | bytes 3076
  83.5 62.1 %collective-permute-start.2 = (bf16[128,256]{1,0:T(8,128)(2,1)S(1)}, bf16[128,256]{1,0:T(8,128)(2,1)S(1)}, u32[]{:S(2)}, u32[]{:S(2)}) collective-permute-start(bf16[128,256]{1,0:T(8,128)(2,1)S(1)} %slice.41), channel_id=1, source_target_pairs={{0,2},{2,4},{4,6},{6,8},{8,10},{10,12},{12,14},{14,16},{16,18},{18... | collective-permute-start | bytes 196616 | tf_op jit(solution)/shard_map/ppermute | solution.py:16
  142.6 4.4 collective-permute-start.1
  387.6 7.8 %collective-permute-start = (bf16[2,768]{1,0:T(2,128)(2,1)S(1)}, bf16[2,768]{1,0:T(2,128)(2,1)S(1)}, u32[]{:S(2)}, u32[]{:S(2)}) collective-permute-start(bf16[2,768]{1,0:T(2,128)(2,1)S(1)} %slice.36), channel_id=1, source_target_pairs={{0,2},{2,4},{4,6},{6,8},{8,10},{10,12},{12,14},{14,16},{16,18},{18... | collective-permute-start | bytes 9224 | tf_op jit(solution)/shard_map/ppermute | solution.py:16
Sparse Core Ops, SparseCore 0:
  8.9 12.2 all-gather.9
  23.9 57.0 all-gather.21
  83.8 56.6 all-gather.19
  143.1 78.3 all-gather.23
  224.1 78.3 all-gather.13
  305.2 78.3 all-gather.15
  386.4 78.3 all-gather.11
  467.5 78.3 all-gather.17
  548.7 78.3 all-gather.25
  632.2 9.9 reduce-scatter.1
where the time goes:
time: 650 us; the launch traced here: 649 us
  waiting for transfers between devices  585 us (90%)
  matrix products  33.3 us (5%)
  between operations  13.7 us (2%)
  starting transfers between devices  9.75 us (2%)
    all_gather x1, waiting for transfers between devices, body(): lax.all_gather(out_conv_w, 'sp', axis=1, tiled=True)  81.2 us
    all_gather x1, waiting for transfers between devices, body(): lax.all_gather(conv_weights[1], 'sp', axis=0, tiled=True)  77.1 us
    all_gather x1, waiting for transfers between devices, body(): lax.all_gather(conv_weights[2], 'sp', axis=0, tiled=True)  76.4 us
    all_gather x1, waiting for transfers between devices, body(): lax.all_gather(attn_weights[0], 'sp', axis=0, tiled=True)  74.4 us
    all_gather x1, waiting for transfers between devices, body(): lax.all_gather(out_attn_w, 'sp', axis=1, tiled=True)  72.8 us
    all_gather x1, waiting for transfers between devices, body(): lax.all_gather(conv_weights[0], 'sp', axis=0, tiled=True)  68.4 us
    all_gather x1, waiting for transfers between devices, body(): lax.all_gather(attn_weights[1], 'sp', axis=0, tiled=True)  57.9 us
    all_gather x1, waiting for transfers between devices, body(): lax.all_gather(attn_weights[2], 'sp', axis=0, tiled=True)  53.9 us
  transfers between devices with their start and end apart: 13, of which 11 were waited for; matrix products, arithmetic and copies ran while one was open for 5% of the time, Pallas kernels for 0%

commit v1 on v0

--- a/solution.py
+++ b/solution.py
@@ -1,6 +1,10 @@
+import functools
+
 import jax
 import jax.numpy as jnp
 from jax import lax
+from jax.experimental import pallas as pl
+from jax.experimental.pallas import tpu as pltpu
 from jax.sharding import PartitionSpec as P
 
 QHEADS = 24
@@ -8,6 +12,8 @@
 HEAD = 64
 TAPS = 3
 WINDOW = 128
+PLANE = 4
+MESH = pl.DeviceIdType.MESH
 
 
 def from_behind(value, axis, steps):
@@ -133,7 +139,484 @@
     return mixed.astype(bf16)
 
 
+def start_to(src, dst, send_sem, recv_sem, target):
+    copy = pltpu.make_async_remote_copy(
+        src_ref=src,
+        dst_ref=dst,
+        send_sem=send_sem,
+        recv_sem=recv_sem,
+        device_id=target,
+        device_id_type=MESH,
+    )
+    copy.start()
+    return copy
+
+
+def place(count):
+    me, core = lax.axis_index("sp"), lax.axis_index("tp")
+    return me, core, me // PLANE, lax.rem(me, PLANE), count // PLANE
+
+
+def greet(me, core, layer, spot, layers):
+    barrier = pltpu.get_barrier_semaphore()
+
+    def signal(target):
+        pl.semaphore_signal(barrier, inc=1, device_id=target, device_id_type=MESH)
+
+    for k in range(1, PLANE):
+        signal({"sp": layer * PLANE + lax.rem(spot + k, PLANE), "tp": core})
+    signal({"sp": me, "tp": 1 - core})
+
+    @pl.when(layer + 1 < layers)
+    def _():
+        signal({"sp": me + PLANE, "tp": core})
+
+    @pl.when(layer > 0)
+    def _():
+        signal({"sp": me - PLANE, "tp": core})
+
+    beside = jnp.where(layer + 1 < layers, 1, 0) + jnp.where(layer > 0, 1, 0)
+    pl.semaphore_wait(barrier, PLANE + beside)
+
+
+def gather_in_kernel(count, tok_ref, w_ref, x_ref, wg_ref, lsem, ws, wr, ts, tr, ds, dr, us, ur, vs, vr):
+    me, core, layer, spot, layers = place(count)
+    rows, half = tok_ref.shape
+    partner = {"sp": me, "tp": 1 - core}
+    above = {"sp": me + PLANE, "tp": core}
+    below = {"sp": me - PLANE, "tp": core}
+    greet(me, core, layer, spot, layers)
+
+    def peer(k):
+        return lax.rem(spot + k, PLANE)
+
+    def source(k):
+        return lax.rem(spot + PLANE - k, PLANE)
+
+    def x_slot(p):
+        return x_ref.at[pl.ds(pl.multiple_of(p * rows, rows), rows), pl.ds(pl.multiple_of(core * half, half), half)]
+
+    def z_copy(up, d, k, own):
+        p = source(k)
+        origin = layer - d if up else layer + d
+        src = w_ref.at[spot] if own else wg_ref.at[origin, p]
+        sems, semr = (us, ur) if up else (vs, vr)
+        return pltpu.make_async_remote_copy(
+            src_ref=src,
+            dst_ref=wg_ref.at[origin, p],
+            send_sem=sems.at[d, k],
+            recv_sem=semr.at[d, k],
+            device_id=above if up else below,
+            device_id_type=MESH,
+        )
+
+    def z_arrive(up, d, k):
+        p = source(k)
+        origin = layer - d if up else layer + d
+        sems, semr = (us, ur) if up else (vs, vr)
+        pltpu.make_async_remote_copy(
+            src_ref=w_ref.at[spot],
+            dst_ref=wg_ref.at[origin, p],
+            send_sem=sems.at[d - 1, k],
+            recv_sem=semr.at[d - 1, k],
+            device_id=above if up else below,
+            device_id_type=MESH,
+        ).wait_recv()
+
+    def both(d, k, own, action):
+        if d < layers - 1:
+            @pl.when((layer + 1 < layers) & (layer >= d))
+            def _():
+                getattr(z_copy(True, d, k, own), action)()
+
+            @pl.when((layer > 0) & (layer + d < layers))
+            def _():
+                getattr(z_copy(False, d, k, own), action)()
+
+    both(0, 0, True, "start")
+    w_copies = [
+        start_to(w_ref.at[peer(k)], wg_ref.at[layer, spot], ws.at[k], wr.at[k], {"sp": layer * PLANE + peer(k), "tp": core})
+        for k in range(1, PLANE)
+    ]
+    t_copies = [
+        start_to(tok_ref, x_slot(spot), ts.at[k], tr.at[k], {"sp": layer * PLANE + peer(k), "tp": core})
+        for k in range(1, PLANE)
+    ]
+    d_copies = [start_to(tok_ref, x_slot(spot), ds.at[0], dr.at[0], partner)]
+    local = [
+        pltpu.make_async_copy(tok_ref, x_slot(spot), lsem.at[0]),
+        pltpu.make_async_copy(w_ref.at[spot], wg_ref.at[layer, spot], lsem.at[1]),
+    ]
+    for copy in local:
+        copy.start()
+    for k in range(1, PLANE):
+        pltpu.make_async_remote_copy(
+            src_ref=w_ref.at[spot], dst_ref=wg_ref.at[layer, source(k)], send_sem=ws.at[k], recv_sem=wr.at[k],
+            device_id=partner, device_id_type=MESH,
+        ).wait_recv()
+        both(0, k, False, "start")
+
+    def receive_layer(d):
+        for k in range(PLANE):
+            @pl.when(layer >= d)
+            def _():
+                z_arrive(True, d, k)
+
+            @pl.when((layer >= d) & (layer + 1 < layers))
+            def _():
+                if d < layers - 1:
+                    z_copy(True, d, k, False).start()
+
+            @pl.when(layer + d < layers)
+            def _():
+                z_arrive(False, d, k)
+
+            @pl.when((layer + d < layers) & (layer > 0))
+            def _():
+                if d < layers - 1:
+                    z_copy(False, d, k, False).start()
+
+    if layers > 1:
+        receive_layer(1)
+    for k in range(1, PLANE):
+        p = source(k)
+        pltpu.make_async_remote_copy(
+            src_ref=tok_ref, dst_ref=x_slot(p), send_sem=ts.at[k], recv_sem=tr.at[k],
+            device_id=partner, device_id_type=MESH,
+        ).wait_recv()
+        d_copies.append(start_to(x_slot(p), x_slot(p), ds.at[k], dr.at[k], partner))
+    for d in range(2, layers):
+        receive_layer(d)
+    for copy in w_copies + t_copies:
+        copy.wait_send()
+    for k, copy in enumerate(d_copies):
+        copy.wait_send()
+        p = source(k)
+        pltpu.make_async_remote_copy(
+            src_ref=tok_ref,
+            dst_ref=x_ref.at[pl.ds(pl.multiple_of(p * rows, rows), rows), pl.ds(pl.multiple_of((1 - core) * half, half), half)],
+            send_sem=ds.at[k], recv_sem=dr.at[k], device_id=partner, device_id_type=MESH,
+        ).wait_recv()
+    for d in range(layers - 1):
+        for k in range(PLANE):
+            both(d, k, d == 0 and k == 0, "wait_send")
+    for copy in local:
+        copy.wait()
+
+
+def gather_in(count, tokens, wblocks):
+    layers = count // PLANE
+    rows, half = tokens.shape
+    _, depth, cols = wblocks.shape
+    dma = pltpu.SemaphoreType.DMA
+    hops = max(layers - 1, 1)
+    return pl.pallas_call(
+        functools.partial(gather_in_kernel, count),
+        out_shape=(
+            jax.ShapeDtypeStruct((PLANE * rows, 2 * half), tokens.dtype),
+            jax.ShapeDtypeStruct((layers, PLANE, depth, cols), wblocks.dtype),
+        ),
+        in_specs=[pl.BlockSpec(memory_space=pltpu.VMEM)] * 2,
+        out_specs=[pl.BlockSpec(memory_space=pl.ANY)] * 2,
+        scratch_shapes=[dma((2,))] + [dma((PLANE,))] * 6 + [dma((hops, PLANE))] * 4,
+        compiler_params=pltpu.CompilerParams(collective_id=0, has_side_effects=True),
+    )(tokens, wblocks)
+
+
+def gather_out_kernel(count, h_ref, o_ref, hg_ref, og_ref, held, lsem, ts, tr, ds, dr, us, ur, vs, vr, es, er, fs):
+    me, core, layer, spot, layers = place(count)
+    width = h_ref.shape[1]
+    cols, depth = o_ref.shape
+    half = cols // 2
+    partner = {"sp": me, "tp": 1 - core}
+    above = {"sp": me + PLANE, "tp": core}
+    below = {"sp": me - PLANE, "tp": core}
+    greet(me, core, layer, spot, layers)
+
+    def peer(k):
+        return lax.rem(spot + k, PLANE)
+
+    def source(k):
+        return lax.rem(spot + PLANE - k, PLANE)
+
+    def h_slot(c, p):
+        return hg_ref.at[:, pl.ds(pl.multiple_of((c * PLANE + p) * width, width), width)]
+
+    def z_copy(up, d, sem_d):
+        origin = layer - d if up else layer + d
+        sems, semr = (us, ur) if up else (vs, vr)
+        return pltpu.make_async_remote_copy(
+            src_ref=o_ref if d == 0 else held.at[origin],
+            dst_ref=held.at[origin],
+            send_sem=sems.at[sem_d],
+            recv_sem=semr.at[sem_d],
+            device_id=above if up else below,
+            device_id_type=MESH,
+        )
+
+    def og_slot(origin, c):
+        return og_ref.at[pl.ds(pl.multiple_of(origin * half, half), half), pl.ds(pl.multiple_of(c * depth, depth), depth)]
+
+    def part(ref, c):
+        return ref.at[pl.ds(pl.multiple_of(c * half, half), half)]
+
+    def pieces(ref, origin, slot):
+        swap = pltpu.make_async_remote_copy(
+            src_ref=part(ref, 1 - core), dst_ref=og_slot(origin, core), send_sem=es.at[slot], recv_sem=er.at[slot],
+            device_id=partner, device_id_type=MESH,
+        )
+        keep = pltpu.make_async_copy(part(ref, core), og_slot(origin, core), fs.at[slot])
+        return swap, keep
+
+    def on_block(up, d, action):
+        origin = layer - d if up else layer + d
+        if d == 0:
+            swap, keep = pieces(o_ref, layer, 0)
+        else:
+            swap, keep = pieces(held.at[origin], origin, d if up else layers - 1 + d)
+        if action == "start":
+            swap.start()
+            keep.start()
+        else:
+            swap.wait_send()
+            keep.wait()
+            pltpu.make_async_remote_copy(
+                src_ref=part(o_ref, core), dst_ref=og_slot(origin, 1 - core), send_sem=es.at[0],
+                recv_sem=er.at[0 if d == 0 else (d if up else layers - 1 + d)],
+                device_id=partner, device_id_type=MESH,
+            ).wait_recv()
+
+    def send(d, action):
+        if d < layers - 1:
+            @pl.when((layer + 1 < layers) & (layer >= d))
+            def _():
+                getattr(z_copy(True, d, d), action)()
+
+            @pl.when((layer > 0) & (layer + d < layers))
+            def _():
+                getattr(z_copy(False, d, d), action)()
+
+    send(0, "start")
+    t_copies = [
+        start_to(h_ref, h_slot(core, spot), ts.at[k], tr.at[k], {"sp": layer * PLANE + peer(k), "tp": core})
+        for k in range(1, PLANE)
+    ]
+    d_copies = [start_to(h_ref, h_slot(core, spot), ds.at[0], dr.at[0], partner)]
+    local = pltpu.make_async_copy(h_ref, h_slot(core, spot), lsem.at[0])
+    local.start()
+    on_block(True, 0, "start")
+
+    def receive_layer(d):
+        @pl.when(layer >= d)
+        def _():
+            z_copy(True, d, d - 1).wait_recv()
+            on_block(True, d, "start")
+
+        @pl.when(layer + d < layers)
+        def _():
+            z_copy(False, d, d - 1).wait_recv()
+            on_block(False, d, "start")
+
+        send(d, "start")
+
+    for d in range(1, max(layers - 1, 1)):
+        receive_layer(d)
+    for k in range(1, PLANE):
+        p = source(k)
+        pltpu.make_async_remote_copy(
+            src_ref=h_ref, dst_ref=h_slot(core, p), send_sem=ts.at[k], recv_sem=tr.at[k],
+            device_id=partner, device_id_type=MESH,
+        ).wait_recv()
+        d_copies.append(start_to(h_slot(core, p), h_slot(core, p), ds.at[k], dr.at[k], partner))
+    if layers > 1:
+        receive_layer(layers - 1)
+    for copy in t_copies:
+        copy.wait_send()
+    for k, copy in enumerate(d_copies):
+        copy.wait_send()
+        pltpu.make_async_remote_copy(
+            src_ref=h_ref, dst_ref=h_slot(1 - core, source(k)), send_sem=ds.at[k], recv_sem=dr.at[k],
+            device_id=partner, device_id_type=MESH,
+        ).wait_recv()
+    on_block(True, 0, "wait")
+    for d in range(layers):
+        send(d, "wait_send")
+    for d in range(1, layers):
+        @pl.when(layer >= d)
+        def _():
+            on_block(True, d, "wait")
+
+        @pl.when(layer + d < layers)
+        def _():
+            on_block(False, d, "wait")
+    local.wait()
+
+
+def gather_out(count, hidden, out_t):
+    layers = count // PLANE
+    rows, width = hidden.shape
+    cols, depth = out_t.shape
+    dma = pltpu.SemaphoreType.DMA
+    hops = max(layers - 1, 1)
+    return pl.pallas_call(
+        functools.partial(gather_out_kernel, count),
+        out_shape=(
+            jax.ShapeDtypeStruct((rows, 2 * PLANE * width), hidden.dtype),
+            jax.ShapeDtypeStruct((layers * cols // 2, 2 * depth), out_t.dtype),
+        ),
+        in_specs=[pl.BlockSpec(memory_space=pltpu.VMEM)] * 2,
+        out_specs=[pl.BlockSpec(memory_space=pl.ANY)] * 2,
+        scratch_shapes=[pltpu.VMEM((layers, cols, depth), out_t.dtype), dma((1,))]
+        + [dma((PLANE,))] * 4
+        + [dma((hops,))] * 4
+        + [dma((2 * layers,))] * 3,
+        compiler_params=pltpu.CompilerParams(collective_id=1, has_side_effects=True),
+    )(hidden, out_t)
+
+
+def exchange_kernel(y_ref, out_ref, lsem, ss, rs):
+    me, core = lax.axis_index("sp"), lax.axis_index("tp")
+    spot = lax.rem(me, PLANE)
+    first = me - spot
+    mine = spot * 2 + core
+    group = 2 * PLANE
+
+    def target(k):
+        other = lax.rem(mine + k, group)
+        return other, {"sp": first + other // 2, "tp": lax.rem(other, 2)}
+
+    barrier = pltpu.get_barrier_semaphore()
+    for k in range(1, group):
+        pl.semaphore_signal(barrier, inc=1, device_id=target(k)[1], device_id_type=MESH)
+    pl.semaphore_wait(barrier, group - 1)
+    copies = []
+    for k in range(1, group):
+        other, device = target(k)
+        copies.append(start_to(y_ref.at[other], out_ref.at[mine], ss.at[k], rs.at[k], device))
+    local = pltpu.make_async_copy(y_ref.at[mine], out_ref.at[mine], lsem.at[0])
+    local.start()
+    for k in range(1, group):
+        copies[k - 1].wait_send()
+        pltpu.make_async_remote_copy(
+            src_ref=y_ref.at[mine], dst_ref=out_ref.at[lax.rem(mine + group - k, group)], send_sem=ss.at[k],
+            recv_sem=rs.at[k], device_id=target(k)[1], device_id_type=MESH,
+        ).wait_recv()
+    local.wait()
+
+
+def exchange(blocks):
+    dma = pltpu.SemaphoreType.DMA
+    return pl.pallas_call(
+        exchange_kernel,
+        out_shape=jax.ShapeDtypeStruct(blocks.shape, blocks.dtype),
+        in_specs=[pl.BlockSpec(memory_space=pltpu.VMEM)],
+        out_specs=pl.BlockSpec(memory_space=pltpu.VMEM),
+        scratch_shapes=[dma((1,)), dma((2 * PLANE,)), dma((2 * PLANE,))],
+        compiler_params=pltpu.CompilerParams(collective_id=2, has_side_effects=True),
+    )(blocks)
+
+
+def window_attention(queries, keys_ext, values_ext, sinks, slopes, offset):
+    f32 = jnp.float32
+    length = queries.shape[0]
+    group = QHEADS // KVHEADS
+    blocks = length // WINDOW
+    qb = queries.reshape(blocks, WINDOW, group, HEAD).transpose(0, 2, 1, 3).reshape(blocks, group * WINDOW, HEAD)
+
+    def pairs(ext):
+        cut = ext.reshape(blocks + 1, WINDOW, HEAD)
+        return jnp.concatenate([cut[:-1], cut[1:]], axis=1)
+
+    kb, vb = pairs(keys_ext), pairs(values_ext)
+    scores = jnp.einsum("bqd,bsd->bqs", qb, kb, preferred_element_type=f32) * HEAD ** (-0.5)
+    scores = scores.reshape(blocks, group, WINDOW, 2 * WINDOW)
+    dist = WINDOW + jnp.arange(WINDOW, dtype=jnp.int32)[:, None] - jnp.arange(2 * WINDOW, dtype=jnp.int32)[None, :]
+    kpos = offset - WINDOW + WINDOW * jnp.arange(blocks, dtype=jnp.int32)[:, None] + jnp.arange(2 * WINDOW, dtype=jnp.int32)[None, :]
+    valid = ((dist >= 0) & (dist < WINDOW))[None] & (kpos >= 0)[:, None, :]
+    scores = scores - slopes[None, :, None, None] * dist.astype(f32)
+    scores = jnp.where(valid[:, None], scores, -1e30)
+    sink = sinks[None, :, None]
+    top = jnp.maximum(jnp.max(scores, axis=-1), sink)
+    expo = jnp.exp(scores - top[..., None])
+    total = jnp.sum(expo, axis=-1) + jnp.exp(sink - top)
+    probs = (expo / total[..., None]).astype(jnp.bfloat16).reshape(blocks, group * WINDOW, 2 * WINDOW)
+    out = jnp.einsum("bqs,bsd->bqd", probs, vb, preferred_element_type=f32)
+    out = out.reshape(blocks, group, WINDOW, HEAD).transpose(0, 2, 1, 3)
+    return out.reshape(length, group * HEAD).astype(jnp.bfloat16)
+
+
+def plane_body(
+    tokens,
+    norm_gain,
+    outer_gate_w,
+    inner_gate_w,
+    signal_w,
+    conv_taps,
+    query_w,
+    key_w,
+    value_w,
+    sink_logits,
+    out_conv_w,
+    out_attn_w,
+):
+    f32 = jnp.float32
+    bf16 = jnp.bfloat16
+    count = lax.axis_size("sp")
+    layers = count // PLANE
+    me, core = lax.axis_index("sp"), lax.axis_index("tp")
+    layer, spot = me // PLANE, lax.rem(me, PLANE)
+    depth = outer_gate_w.shape[0]
+    chans = outer_gate_w.shape[1] // PLANE
+    wide = query_w.shape[1] // PLANE
+    group = QHEADS // KVHEADS
+
+    def cut(weight):
+        return weight.reshape(depth, PLANE, -1).transpose(1, 0, 2)
+
+    wblocks = jnp.concatenate(
+        [cut(w) for w in (outer_gate_w, inner_gate_w, signal_w, query_w, key_w, value_w)], axis=2
+    )
+    x, weights = gather_in(count, tokens, wblocks)
+    x32 = x.astype(f32)
+    normed = (
+        x32 * lax.rsqrt(jnp.mean(x32 * x32, axis=-1, keepdims=True) + 1e-06) * norm_gain
+    ).astype(bf16)
+    proj = jnp.dot(normed, weights.reshape(x.shape[1], -1), preferred_element_type=f32).astype(bf16)
+    outer, inner, signal = (proj[:, i * chans : (i + 1) * chans] for i in range(3))
+    queries = proj[:, 3 * chans : 3 * chans + wide]
+    keys = proj[:, 3 * chans + wide : 3 * chans + wide + HEAD]
+    values = proj[:, 3 * chans + wide + HEAD :]
+    length = proj.shape[0]
+    gated = (inner.astype(f32) * signal.astype(f32)).astype(bf16)
+    before = from_behind(gated[length - TAPS + 1 :], "sp", PLANE)
+    kv_before = from_behind(proj[length - WINDOW :, 3 * chans + wide :], "sp", PLANE)
+    taps = lax.dynamic_slice_in_dim(conv_taps, spot * chans, chans, 1)
+    conv_out = convolve(gated, before, outer, taps)
+    keys_ext = jnp.concatenate([kv_before[:, :HEAD], keys], axis=0)
+    values_ext = jnp.concatenate([kv_before[:, HEAD:], values], axis=0)
+    head = (core * PLANE + spot) * group + 1 + jnp.arange(group, dtype=jnp.int32)
+    slopes = jnp.exp2(-8.0 * head.astype(f32) / QHEADS)
+    sinks = lax.dynamic_slice_in_dim(sink_logits, spot * group, group, 0)
+    attn_out = window_attention(queries, keys_ext, values_ext, sinks, slopes, layer * length)
+    hidden = jnp.concatenate([conv_out, attn_out], axis=1)
+    cols = out_conv_w.shape[1]
+    out_t = jnp.concatenate(
+        [out_conv_w.reshape(PLANE, chans, cols), out_attn_w.reshape(PLANE, wide, cols)], axis=1
+    ).reshape(-1, cols).T
+    hidden_all, out_all = gather_out(count, hidden, out_t)
+    result = lax.dot_general(
+        hidden_all, out_all, (((1,), (1,)), ((), ())), preferred_element_type=f32
+    ).astype(bf16)
+    swapped = exchange(result.reshape(2 * PLANE, length // (2 * PLANE), -1))
+    rows = length // (2 * PLANE)
+    swapped = swapped.reshape(PLANE, 2, rows, layers, cols // 2).transpose(2, 3, 0, 1, 4)
+    return swapped.reshape(rows, -1)
+
+
 def solution(mesh):
+    kv_local = KVHEADS // mesh.shape["tp"]
+    fits = mesh.shape["tp"] == 2 and kv_local == PLANE and mesh.shape["sp"] % PLANE == 0
+    chosen = plane_body if fits else body
     in_specs = (
         P("sp", "tp"),
         P(),
@@ -149,4 +632,4 @@
         P("tp", "sp"),
     )
     out_specs = P(("sp", "tp"), None)
-    return jax.shard_map(body, mesh=mesh, in_specs=in_specs, out_specs=out_specs, check_vma=False)
+    return jax.shard_map(chosen, mesh=mesh, in_specs=in_specs, out_specs=out_specs, check_vma=False)

time: 650 us -> 239 us (0.37)
  waiting for transfers between devices: 585 us -> 0.01 us
  Pallas kernels: 0 us -> 161 us
  local copies, waits for them, and re-layouts: 2.11 us -> 37.8 us
  between operations: 13.7 us -> 0.28 us
  matrix products: 33.3 us -> 21.1 us
  other arithmetic: 4.75 us -> 13.2 us
    all_gather x9 -> x0, waiting for transfers between devices: 568 us -> none  [the longest x1 81.2 us: body(): lax.all_gather(out_conv_w, 'sp', axis=1, tiled=True)]
    pallas_call x0 -> x3, Pallas kernels: none -> 161 us  [the longest x1 95.4 us: gather_in(): pl.pallas_call(functools.partial(gather_in_kernel, count), out_shape=(jax...]
    dot_general x9 -> x4, matrix products: 33.3 us -> 21.1 us  [the longest x1 8.88 us: plane_body(): jnp.dot(normed, weights.reshape(x.shape[1], -1), preferred_element_type=f32)]
    reshape x0 -> x10, local copies, waits for them, and re-layouts: none -> 12.1 us  [the longest x6 5.72 us: cut(): return weight.reshape(depth, PLANE, -1).transpose(1, 0, 2)]
    reduce_scatter x1 -> x0, waiting for transfers between devices: 10.1 us -> none  [body(): lax.psum_scatter((result + jnp.dot(attn_out, attn_whole, preferred_elemen...]
    slice x3 -> x10, local copies, waits for them, and re-layouts: 0.02 us -> 9.28 us  [the longest x4 3.43 us: pairs(): return jnp.concatenate([cut[:-1], cut[1:]], axis=1)]
  transfers between devices with their start and end apart: 13 -> 2, of which waited for: 11 -> 0; matrix products, arithmetic and copies ran while one was open for 5% -> 10% of each run, Pallas kernels for 0% -> 0%
where the time goes in v1:
time: 239 us
  Pallas kernels  161 us (67%)
  local copies, waits for them, and re-layouts  37.8 us (16%)
  matrix products  21.1 us (9%)
  other arithmetic  13.2 us (6%)
  starting transfers between devices  4.89 us (2%)
    pallas_call x1, Pallas kernels, gather_in(): pl.pallas_call(functools.partial(gather_in_kernel, count), out_shape=(jax...  95.4 us
    pallas_call x1, Pallas kernels, gather_out(): pl.pallas_call(functools.partial(gather_out_kernel, count), out_shape=(ja...  48.2 us
    pallas_call x1, Pallas kernels, exchange(): pl.pallas_call(exchange_kernel, out_shape=jax.ShapeDtypeStruct(blocks.sha...  17.8 us
    dot_general x1, matrix products, plane_body(): jnp.dot(normed, weights.reshape(x.shape[1], -1), preferred_element_type=f32)  8.88 us
    dot_general x1, matrix products, plane_body(): lax.dot_general(hidden_all, out_all, (((1,), (1,)), ((), ())), preferred_...  7.8 us
    reshape x6, local copies, waits for them, and re-layouts, cut(): return weight.reshape(depth, PLANE, -1).transpose(1, 0, 2)  5.72 us
    ppermute x2, starting transfers between devices, from_behind(): lax.ppermute(value, axis, [(source, source + steps) for source in range(i...  4.89 us
  transfers between devices with their start and end apart: 2, of which 0 were waited for; matrix products, arithmetic and copies ran while one was open for 10% of the time, Pallas kernels for 0%

profile of v1, /device:TPU:1, one launch (start us, length us, event | category | flops | bytes accessed | tf_op | source)
XLA Modules:
  0.0 238.6 jit_solution(5753953774758908151)
XLA Ops:
  0.0 1.4 reshape.192
  1.4 1.3 reshape.193
  2.7 1.3 reshape.190
  4.1 1.3 reshape.191
  7.1 2.2 concatenate.24.w_ref
  9.3 95.4 %shard_map.118 = (bf16[1024,3072]{1,0:T(8,128)(2,1)}, bf16[4,4,192,896]{3,2,1,0:T(8,128)(2,1)}) custom-call(bf16[256,1536]{1,0:T(8,128)(2,1)} %tok_ref.1, bf16[4,192,896]{2,1,0:T(8,128)(2,1)} %concatenate.24.w_ref), custom_call_target="tpu_custom_call" | custom-call | tf_op jit(solution)/shard_map/pallas_call | solution.py:313
  104.7 4.2 %fusion = f32[1024]{0:T(1024)S(1)} fusion(bf16[1024,3072]{1,0:T(8,128)(2,1)} %get-tuple-element.9), kind=kLoop, calls=%fused_computation.2 | loop fusion | flops 9436160 | bytes 6295552 | tf_op jit(solution)/shard_map/reduce_sum | solution.py:582
  109.3 8.9 %fusion.8 = bf16[1024,896]{1,0:T(8,128)(2,1)S(1)} fusion(bf16[3072,896]{1,0:T(8,128)(2,1)} %bitcast.87, bf16[1024,3072]{1,0:T(8,128)(2,1)S(1)} %copy-done.1, f32[3072]{0:T(1024)S(1)} %copy-done.9, f32[1024]{0:T(1024)S(1)} %add_rsqrt_fusion), kind=kOutput, calls=%fused_computation.12 | convolution fusion | flops 5650644992 | bytes 13647872 | tf_op jit(solution)/shard_map/dot_general | solution.py:584
  119.1 1.8 collective-permute-start
  121.5 3.1 %collective-permute-start.1 = (bf16[128,128]{1,0:T(8,128)(2,1)}, bf16[128,128]{1,0:T(8,128)(2,1)}, u32[]{:S(2)}, u32[]{:S(2)}) collective-permute-start(bf16[128,128]{1,0:T(8,128)(2,1)} %slice.97), channel_id=1, source_target_pairs={{0,8},{2,10},{4,12},{6,14},{8,16},{10,18},{12,20},{14,22},{16,24},... | collective-permute-start | bytes 98312 | tf_op jit(solution)/shard_map/ppermute | solution.py:22
  124.9 1.0 slice.100
  126.5 1.8 copy.36
  129.1 1.1 reshape.199
  130.2 2.1 reshape.200
  133.1 1.6 pad_maximum_fusion.1
  135.6 1.9 copy.35
  138.3 2.0 copy.31
  140.3 1.1 copy.47
  141.4 1.1 copy.32
  142.5 2.0 reshape.198
  147.1 1.2 fusion.15
  148.3 1.5 fusion.30
  150.7 2.3 fusion.31
  155.5 1.1 copy.37
  156.6 2.1 fusion.12
  158.7 1.4 convert_element_type.73
  160.8 1.2 pad_maximum_fusion.h_ref
  162.0 48.2 %shard_map.119 = (bf16[1024,3072]{1,0:T(8,128)(2,1)}, bf16[384,3072]{1,0:T(8,128)(2,1)}) custom-call(bf16[1024,384]{1,0:T(8,128)(2,1)} %pad_maximum_fusion.h_ref, bf16[192,1536]{1,0:T(8,128)(2,1)} %bitcast.68), custom_call_target="tpu_custom_call" | custom-call | tf_op jit(solution)/shard_map/pallas_call | solution.py:461
  210.2 7.8 %convolution_convert_fusion = bf16[1024,384]{1,0:T(8,128)(2,1)} fusion(bf16[1024,3072]{1,0:T(8,128)(2,1)} %get-tuple-element.11, bf16[384,3072]{1,0:T(8,128)(2,1)} %get-tuple-element.12), kind=kOutput, calls=%fused_computation.14 | convolution fusion | flops 2416312320 | bytes 9437184 | tf_op jit(solution)/shard_map/dot_general | solution.py:607
  218.0 17.8 %shard_map.120 = bf16[8,128,384]{2,1,0:T(8,128)(2,1)} custom-call(bf16[8,128,384]{2,1,0:T(8,128)(2,1)} %bitcast.81), custom_call_target="tpu_custom_call" | custom-call | tf_op jit(solution)/shard_map/pallas_call | solution.py:509
  235.8 1.5 copy.42
  237.4 1.2 copy.44
  (60 shorter events, 14.3 us)
Async XLA Ops:
  0.0 128.3 %copy-start = (f32[12]{0:T(128)S(1)}, f32[12]{0:T(128)}, u32[]{:S(2)}) copy-start(f32[12]{0:T(128)} %param.21) | copy-start | bytes 148
  0.0 6.6 %copy-start.7 = (bf16[192,256]{1,0:T(8,128)(2,1)S(1)}, bf16[192,256]{1,0:T(8,128)(2,1)}, u32[]{:S(2)}) copy-start(bf16[192,256]{1,0:T(8,128)(2,1)} %param.20) | copy-start | bytes 294916
  104.7 4.6 %copy-start.1 = (bf16[1024,3072]{1,0:T(8,128)(2,1)S(1)}, bf16[1024,3072]{1,0:T(8,128)(2,1)}, u32[]{:S(2)}) copy-start(bf16[1024,3072]{1,0:T(8,128)(2,1)} %get-tuple-element.9) | copy-start | bytes 18874372
  104.7 4.6 %copy-start.9 = (f32[3072]{0:T(1024)S(1)}, f32[3072]{0:T(1024)}, u32[]{:S(2)}) copy-start(f32[3072]{0:T(1024)} %param.13) | copy-start | bytes 36868
  118.2 10.9 %copy-start.4 = (bf16[768,192]{0,1:T(8,128)(2,1)S(1)}, bf16[768,192]{0,1:T(8,128)(2,1)}, u32[]{:S(2)}) copy-start(bf16[768,192]{0,1:T(8,128)(2,1)} %param.22) | copy-start | bytes 884740
  119.1 27.2 %collective-permute-start = (bf16[2,192]{1,0:T(2,128)(2,1)}, bf16[2,192]{1,0:T(2,128)(2,1)}, u32[]{:S(2)}, u32[]{:S(2)}) collective-permute-start(bf16[2,192]{1,0:T(2,128)(2,1)} %slice.93), channel_id=1, source_target_pairs={{0,8},{2,10},{4,12},{6,14},{8,16},{10,18},{12,20},{14,22},{16,24},... | collective-permute-start | bytes 2312 | tf_op jit(solution)/shard_map/ppermute | solution.py:22
  121.5 26.8 %collective-permute-start.1 = (bf16[128,128]{1,0:T(8,128)(2,1)}, bf16[128,128]{1,0:T(8,128)(2,1)}, u32[]{:S(2)}, u32[]{:S(2)}) collective-permute-start(bf16[128,128]{1,0:T(8,128)(2,1)} %slice.97), channel_id=1, source_target_pairs={{0,8},{2,10},{4,12},{6,14},{8,16},{10,18},{12,20},{14,22},{16,24},... | collective-permute-start | bytes 98312 | tf_op jit(solution)/shard_map/ppermute | solution.py:22
  146.3 4.4 %copy-start.3 = (bf16[8,128,64]{1,2,0:T(8,128)(2,1)S(1)}, bf16[8,128,64]{1,2,0:T(8,128)(2,1)}, u32[]{:S(2)}) copy-start(bf16[8,128,64]{1,2,0:T(8,128)(2,1)} %copy.34) | copy-start | bytes 393220
  150.7 3.5 %copy-start.8 = (f32[384]{0:T(512)S(1)}, f32[384]{0:T(512)}, u32[]{:S(2)}) copy-start(f32[384]{0:T(512)} %broadcast_bitcast_fusion) | copy-start | bytes 4612
  150.7 4.1 %copy-start.6 = (bf16[128,64]{1,0:T(8,128)(2,1)S(1)}, bf16[128,64]{1,0:T(8,128)(2,1)}, u32[]{:S(2)}) copy-start(bf16[128,64]{1,0:T(8,128)(2,1)} %get-tuple-element.15) | copy-start | bytes 49156
  153.0 3.6 %copy-start.5 = (bf16[8,128,64]{1,2,0:T(8,128)(2,1)S(1)}, bf16[8,128,64]{1,2,0:T(8,128)(2,1)}, u32[]{:S(2)}) copy-start(bf16[8,128,64]{1,2,0:T(8,128)(2,1)} %copy.38) | copy-start | bytes 393220
  158.7 2.1 copy-start.2

commit v2 on v1

--- a/solution.py
+++ b/solution.py
@@ -516,33 +516,92 @@
     )(blocks)
 
 
-def window_attention(queries, keys_ext, values_ext, sinks, slopes, offset):
-    f32 = jnp.float32
-    length = queries.shape[0]
-    group = QHEADS // KVHEADS
-    blocks = length // WINDOW
-    qb = queries.reshape(blocks, WINDOW, group, HEAD).transpose(0, 2, 1, 3).reshape(blocks, group * WINDOW, HEAD)
-
-    def pairs(ext):
-        cut = ext.reshape(blocks + 1, WINDOW, HEAD)
-        return jnp.concatenate([cut[:-1], cut[1:]], axis=1)
-
-    kb, vb = pairs(keys_ext), pairs(values_ext)
-    scores = jnp.einsum("bqd,bsd->bqs", qb, kb, preferred_element_type=f32) * HEAD ** (-0.5)
-    scores = scores.reshape(blocks, group, WINDOW, 2 * WINDOW)
-    dist = WINDOW + jnp.arange(WINDOW, dtype=jnp.int32)[:, None] - jnp.arange(2 * WINDOW, dtype=jnp.int32)[None, :]
-    kpos = offset - WINDOW + WINDOW * jnp.arange(blocks, dtype=jnp.int32)[:, None] + jnp.arange(2 * WINDOW, dtype=jnp.int32)[None, :]
-    valid = ((dist >= 0) & (dist < WINDOW))[None] & (kpos >= 0)[:, None, :]
-    scores = scores - slopes[None, :, None, None] * dist.astype(f32)
-    scores = jnp.where(valid[:, None], scores, -1e30)
-    sink = sinks[None, :, None]
-    top = jnp.maximum(jnp.max(scores, axis=-1), sink)
-    expo = jnp.exp(scores - top[..., None])
-    total = jnp.sum(expo, axis=-1) + jnp.exp(sink - top)
-    probs = (expo / total[..., None]).astype(jnp.bfloat16).reshape(blocks, group * WINDOW, 2 * WINDOW)
-    out = jnp.einsum("bqs,bsd->bqd", probs, vb, preferred_element_type=f32)
-    out = out.reshape(blocks, group, WINDOW, HEAD).transpose(0, 2, 1, 3)
-    return out.reshape(length, group * HEAD).astype(jnp.bfloat16)
+def pack_kernel(*refs):
+    *weights, out_ref = refs
+    for p in range(PLANE):
+        pieces = []
+        for ref in weights:
+            width = ref.shape[1] // PLANE
+            pieces.append(ref[:, p * width : (p + 1) * width])
+        out_ref[p] = jnp.concatenate(pieces, axis=1)
+
+
+def pack(weights):
+    depth = weights[0].shape[0]
+    cols = sum(w.shape[1] for w in weights) // PLANE
+    return pl.pallas_call(
+        pack_kernel,
+        out_shape=jax.ShapeDtypeStruct((PLANE, depth, cols), weights[0].dtype),
+        in_specs=[pl.BlockSpec(memory_space=pltpu.VMEM)] * len(weights),
+        out_specs=pl.BlockSpec(memory_space=pltpu.VMEM),
+    )(*weights)
+
+
+def mixer_kernel(chans, wide, slopes_ref, sinks_ref, offset_ref, proj_ref, before_ref, kv_before_ref, taps_ref, out_ref, ext, gext):
+    f32, bf16 = jnp.float32, jnp.bfloat16
+    length = proj_ref.shape[0]
+    group = wide // HEAD
+    front = 8
+    ext[0:WINDOW] = kv_before_ref[...]
+    ext[WINDOW:] = proj_ref[:, 3 * chans + wide :]
+    gext[0:front] = jnp.concatenate(
+        [jnp.zeros((front - TAPS + 1, chans), f32), before_ref[...].astype(f32)], axis=0
+    )
+    row = lax.broadcasted_iota(jnp.int32, (WINDOW, 2 * WINDOW), 0)
+    col = lax.broadcasted_iota(jnp.int32, (WINDOW, 2 * WINDOW), 1)
+    dist = WINDOW + row - col
+    near = (dist >= 0) & (dist < WINDOW)
+    far = dist.astype(f32)
+
+    def block(i, carry):
+        start = pl.multiple_of(i * WINDOW, WINDOW)
+        rows = pl.ds(start, WINDOW)
+        chunk = proj_ref[rows, :]
+        inner = chunk[:, chans : 2 * chans].astype(f32)
+        signal = chunk[:, 2 * chans : 3 * chans].astype(f32)
+        gext[pl.ds(pl.multiple_of(start + front, 8), WINDOW), :] = (inner * signal).astype(bf16).astype(f32)
+        window = gext[pl.ds(start, WINDOW + front), :]
+        conv = sum(
+            taps_ref[k : k + 1, :] * window[front - TAPS + 1 + k : front - TAPS + 1 + k + WINDOW]
+            for k in range(TAPS)
+        )
+        pieces = [(chunk[:, :chans].astype(f32) * conv).astype(bf16)]
+        kv = ext[pl.ds(start, 2 * WINDOW), :]
+        keys, values = kv[:, :HEAD], kv[:, HEAD:]
+        valid = near & (offset_ref[0] + start - WINDOW + col >= 0)
+        for g in range(group):
+            first = 3 * chans + g * HEAD
+            scores = lax.dot_general(
+                chunk[:, first : first + HEAD], keys, (((1,), (1,)), ((), ())), preferred_element_type=f32
+            ) * HEAD ** (-0.5)
+            scores = jnp.where(valid, scores - slopes_ref[g] * far, -1e30)
+            sink = sinks_ref[g]
+            top = jnp.maximum(jnp.max(scores, axis=1, keepdims=True), sink)
+            expo = jnp.exp(scores - top)
+            total = jnp.sum(expo, axis=1, keepdims=True) + jnp.exp(sink - top)
+            probs = (expo / total).astype(bf16)
+            pieces.append(jnp.dot(probs, values, preferred_element_type=f32).astype(bf16))
+        out_ref[rows, :] = jnp.concatenate(pieces, axis=1)
+        return carry
+
+    lax.fori_loop(0, length // WINDOW, block, 0)
+
+
+def mixer(proj, before, kv_before, taps, slopes, sinks, offset, wide):
+    length = proj.shape[0]
+    chans = taps.shape[1]
+    smem = pl.BlockSpec(memory_space=pltpu.SMEM)
+    vmem = pl.BlockSpec(memory_space=pltpu.VMEM)
+    return pl.pallas_call(
+        functools.partial(mixer_kernel, chans, wide),
+        out_shape=jax.ShapeDtypeStruct((length, chans + wide), jnp.bfloat16),
+        in_specs=[smem] * 3 + [vmem] * 4,
+        out_specs=vmem,
+        scratch_shapes=[
+            pltpu.VMEM((WINDOW + length, 2 * HEAD), jnp.bfloat16),
+            pltpu.VMEM((8 + length, chans), jnp.float32),
+        ],
+    )(slopes, sinks, jnp.reshape(offset, (1,)), proj, before, kv_before, taps)
 
 
 def plane_body(
@@ -565,40 +624,26 @@
     layers = count // PLANE
     me, core = lax.axis_index("sp"), lax.axis_index("tp")
     layer, spot = me // PLANE, lax.rem(me, PLANE)
-    depth = outer_gate_w.shape[0]
     chans = outer_gate_w.shape[1] // PLANE
     wide = query_w.shape[1] // PLANE
     group = QHEADS // KVHEADS
 
-    def cut(weight):
-        return weight.reshape(depth, PLANE, -1).transpose(1, 0, 2)
-
-    wblocks = jnp.concatenate(
-        [cut(w) for w in (outer_gate_w, inner_gate_w, signal_w, query_w, key_w, value_w)], axis=2
-    )
+    wblocks = pack((outer_gate_w, inner_gate_w, signal_w, query_w, key_w, value_w))
     x, weights = gather_in(count, tokens, wblocks)
     x32 = x.astype(f32)
     normed = (
         x32 * lax.rsqrt(jnp.mean(x32 * x32, axis=-1, keepdims=True) + 1e-06) * norm_gain
     ).astype(bf16)
     proj = jnp.dot(normed, weights.reshape(x.shape[1], -1), preferred_element_type=f32).astype(bf16)
-    outer, inner, signal = (proj[:, i * chans : (i + 1) * chans] for i in range(3))
-    queries = proj[:, 3 * chans : 3 * chans + wide]
-    keys = proj[:, 3 * chans + wide : 3 * chans + wide + HEAD]
-    values = proj[:, 3 * chans + wide + HEAD :]
     length = proj.shape[0]
-    gated = (inner.astype(f32) * signal.astype(f32)).astype(bf16)
-    before = from_behind(gated[length - TAPS + 1 :], "sp", PLANE)
+    last = proj[length - TAPS + 1 :, chans : 3 * chans].astype(f32)
+    before = from_behind((last[:, :chans] * last[:, chans:]).astype(bf16), "sp", PLANE)
     kv_before = from_behind(proj[length - WINDOW :, 3 * chans + wide :], "sp", PLANE)
     taps = lax.dynamic_slice_in_dim(conv_taps, spot * chans, chans, 1)
-    conv_out = convolve(gated, before, outer, taps)
-    keys_ext = jnp.concatenate([kv_before[:, :HEAD], keys], axis=0)
-    values_ext = jnp.concatenate([kv_before[:, HEAD:], values], axis=0)
     head = (core * PLANE + spot) * group + 1 + jnp.arange(group, dtype=jnp.int32)
     slopes = jnp.exp2(-8.0 * head.astype(f32) / QHEADS)
     sinks = lax.dynamic_slice_in_dim(sink_logits, spot * group, group, 0)
-    attn_out = window_attention(queries, keys_ext, values_ext, sinks, slopes, layer * length)
-    hidden = jnp.concatenate([conv_out, attn_out], axis=1)
+    hidden = mixer(proj, before, kv_before, taps, slopes, sinks, layer * length, wide)
     cols = out_conv_w.shape[1]
     out_t = jnp.concatenate(
         [out_conv_w.reshape(PLANE, chans, cols), out_attn_w.reshape(PLANE, wide, cols)], axis=1

time: 239 us -> 209 us (0.87)
  local copies, waits for them, and re-layouts: 37.8 us -> 6.67 us
  Pallas kernels: 161 us -> 175 us
  other arithmetic: 13.2 us -> 5.41 us
  matrix products: 21.1 us -> 16.7 us
    pallas_call x0 -> x2, Pallas kernels: none -> 13.2 us  [the longest x1 10.4 us: mixer(): pl.pallas_call(functools.partial(mixer_kernel, chans, wide), out_shape=ja...]
    slice x10 -> x0, local copies, waits for them, and re-layouts: 9.57 us -> none  [the longest x4 3.43 us: pairs(): return jnp.concatenate([cut[:-1], cut[1:]], axis=1)]
    reshape x7 -> x0, local copies, waits for them, and re-layouts: 7.76 us -> none  [the longest x6 5.72 us: cut(): return weight.reshape(depth, PLANE, -1).transpose(1, 0, 2)]
    dot_general x2 -> x0, matrix products: 4.44 us -> none  [the longest x1 2.3 us: window_attention(): jnp.einsum('bqd,bsd->bqs', qb, kb, preferred_element_type=f32)]
  transfers between devices with their start and end apart: 2 -> 2, of which waited for: 0 -> 0; matrix products, arithmetic and copies ran while one was open for 10% -> 2% of each run, Pallas kernels for 0% -> 0%
where the time goes in v2:
time: 209 us; the launch traced here: 208 us
  Pallas kernels  175 us (84%)
  matrix products  16.7 us (8%)
  local copies, waits for them, and re-layouts  6.67 us (3%)
  other arithmetic  5.41 us (3%)
  starting transfers between devices  4.29 us (2%)
    pallas_call x1, Pallas kernels, gather_in(): pl.pallas_call(functools.partial(gather_in_kernel, count), out_shape=(jax...  95.4 us
    pallas_call x1, Pallas kernels, gather_out(): pl.pallas_call(functools.partial(gather_out_kernel, count), out_shape=(ja...  48.6 us
    pallas_call x1, Pallas kernels, exchange(): pl.pallas_call(exchange_kernel, out_shape=jax.ShapeDtypeStruct(blocks.sha...  17.8 us
    pallas_call x1, Pallas kernels, mixer(): pl.pallas_call(functools.partial(mixer_kernel, chans, wide), out_shape=ja...  10.4 us
    dot_general x1, matrix products, plane_body(): jnp.dot(normed, weights.reshape(x.shape[1], -1), preferred_element_type=f32)  8.95 us
    dot_general x1, matrix products, plane_body(): lax.dot_general(hidden_all, out_all, (((1,), (1,)), ((), ())), preferred_...  7.79 us
    ppermute x2, starting transfers between devices, from_behind(): lax.ppermute(value, axis, [(source, source + steps) for source in range(i...  4.29 us
    reduce_sum x1, other arithmetic, plane_body(): jnp.mean(x32 * x32, axis=-1, keepdims=True) + 1e-06  4.23 us
  transfers between devices with their start and end apart: 2, of which 0 were waited for; matrix products, arithmetic and copies ran while one was open for 2% of the time, Pallas kernels for 0%

profile of v2, /device:TPU:1, one launch (start us, length us, event | category | flops | bytes accessed | tf_op | source)
XLA Modules:
  0.0 208.2 jit_solution(11206009281525504125)
XLA Ops:
  0.0 0.0 copy-start
  0.0 2.8 %shard_map.118.w_ref = bf16[4,192,896]{2,1,0:T(8,128)(2,1)} custom-call(bf16[192,768]{1,0:T(8,128)(2,1)} %refs_0_.1, bf16[192,768]{1,0:T(8,128)(2,1)} %refs_1_.1, bf16[192,768]{1,0:T(8,128)(2,1)} %refs_2_.1, bf16[192,768]{1,0:T(8,128)(2,1)} %refs_3_.1, bf16[192,256]{1,0:T(8,128)(2,1)} %refs_4_.1, bf16[192,256]{1,0:T(8,128)(2,1)} %refs_5_.1), custom_call_target="tpu_custom_call" | custom-call | tf_op jit(solution)/shard_map/pallas_call | solution.py:532
  2.8 95.4 %shard_map.119 = (bf16[1024,3072]{1,0:T(8,128)(2,1)}, bf16[4,4,192,896]{3,2,1,0:T(8,128)(2,1)}) custom-call(bf16[256,1536]{1,0:T(8,128)(2,1)} %tok_ref.1, bf16[4,192,896]{2,1,0:T(8,128)(2,1)} %shard_map.118.w_ref), custom_call_target="tpu_custom_call" | custom-call | tf_op jit(solution)/shard_map/pallas_call | solution.py:313
  98.2 0.0 copy-start.1
  98.2 4.2 %fusion = f32[1024]{0:T(1024)S(1)} fusion(bf16[1024,3072]{1,0:T(8,128)(2,1)} %get-tuple-element.9), kind=kLoop, calls=%fused_computation.2 | loop fusion | flops 9436160 | bytes 6295552 | tf_op jit(solution)/shard_map/reduce_sum | solution.py:635
  102.5 0.0 copy-done.7
  102.5 0.3 copy-done.1
  102.8 9.0 %fusion.7.proj_ref = bf16[1024,896]{1,0:T(8,128)(2,1)S(1)} fusion(bf16[3072,896]{1,0:T(8,128)(2,1)} %bitcast.25, bf16[1024,3072]{1,0:T(8,128)(2,1)S(1)} %copy-done.1, f32[3072]{0:T(1024)S(1)} %copy-done.7, f32[1024]{0:T(1024)S(1)} %add_rsqrt_fusion), kind=kOutput, calls=%fused_computation.8 | convolution fusion | flops 5650644992 | bytes 13647872 | tf_op jit(solution)/shard_map/dot_general | solution.py:637
  111.8 0.0 copy-start.2
  111.8 0.1 slice_convert_fusion
  111.9 0.1 fusion.10
  111.9 1.3 collective-permute-start
  113.2 3.0 %collective-permute-start.1 = (bf16[128,128]{1,0:T(8,128)(2,1)S(1)}, bf16[128,128]{1,0:T(8,128)(2,1)S(1)}, u32[]{:S(2)}, u32[]{:S(2)}) collective-permute-start(bf16[128,128]{1,0:T(8,128)(2,1)S(1)} %slice.19), channel_id=1, source_target_pairs={{0,8},{2,10},{4,12},{6,14},{8,16},{10,18},{12,20},{14,22},{16,24},... | collective-permute-start | bytes 98312 | tf_op jit(solution)/shard_map/ppermute | solution.py:22
  116.3 0.0 copy-done.3
  116.3 0.4 reshape.36
  116.6 0.4 reshape.35
  117.0 0.7 constant_dynamic-slice_fusion.taps_ref
  117.7 0.5 pad_maximum_fusion
  118.2 0.5 multiply_exponential_fusion.slopes_ref
  118.7 1.0 copy.17
  119.7 0.6 dynamic_slice.6.sinks_ref
  120.3 0.0 collective-permute-done.before_ref
  120.3 0.0 collective-permute-done.1.kv_before_ref
  120.3 0.6 copy-done.6
  120.9 0.0 copy-done.5
  120.9 10.4 %shard_map.120.h_ref = bf16[1024,384]{1,0:T(8,128)(2,1)} custom-call(f32[3]{0:T(128)} %multiply_exponential_fusion.slopes_ref, f32[3]{0:T(128)} %dynamic_slice.6.sinks_ref, s32[1]{0:T(128)} %bitcast.offset_ref, bf16[1024,896]{1,0:T(8,128)(2,1)} %copy-done.2, bf16[2,192]{1,0:T(2,128)(2,1)} %copy-done.6, bf16[128,128]{1,0:T(8,128)(2,1)} %copy-done.5, ...), custom_call_target="tpu_custom_call" | custom-call | tf_op jit(solution)/shard_map/pallas_call | solution.py:595
  131.3 48.6 %shard_map.121 = (bf16[1024,3072]{1,0:T(8,128)(2,1)}, bf16[384,3072]{1,0:T(8,128)(2,1)}) custom-call(bf16[1024,384]{1,0:T(8,128)(2,1)} %shard_map.120.h_ref, bf16[192,1536]{1,0:T(8,128)(2,1)} %bitcast.22), custom_call_target="tpu_custom_call" | custom-call | tf_op jit(solution)/shard_map/pallas_call | solution.py:461
  179.9 7.8 %convolution_convert_fusion = bf16[1024,384]{1,0:T(8,128)(2,1)} fusion(bf16[1024,3072]{1,0:T(8,128)(2,1)} %get-tuple-element.11, bf16[384,3072]{1,0:T(8,128)(2,1)} %get-tuple-element.12), kind=kOutput, calls=%fused_computation.9 | convolution fusion | flops 2416312320 | bytes 9437184 | tf_op jit(solution)/shard_map/dot_general | solution.py:652
  187.7 17.8 %shard_map.122 = bf16[8,128,384]{2,1,0:T(8,128)(2,1)} custom-call(bf16[8,128,384]{2,1,0:T(8,128)(2,1)} %bitcast.24), custom_call_target="tpu_custom_call" | custom-call | tf_op jit(solution)/shard_map/pallas_call | solution.py:509
  205.5 1.5 copy.14
  207.0 0.1 copy.15
  207.1 1.2 copy.16
  (12 shorter events, 0.0 us)
Async XLA Ops:
  0.0 117.0 %copy-start = (f32[3,768]{1,0:T(4,128)S(1)}, f32[3,768]{1,0:T(4,128)}, u32[]{:S(2)}) copy-start(f32[3,768]{1,0:T(4,128)} %param.17) | copy-start | bytes 27652
  0.0 102.5 %copy-start.7 = (f32[3072]{0:T(1024)S(1)}, f32[3072]{0:T(1024)}, u32[]{:S(2)}) copy-start(f32[3072]{0:T(1024)} %param.13) | copy-start | bytes 36868
  98.2 4.6 %copy-start.1 = (bf16[1024,3072]{1,0:T(8,128)(2,1)S(1)}, bf16[1024,3072]{1,0:T(8,128)(2,1)}, u32[]{:S(2)}) copy-start(bf16[1024,3072]{1,0:T(8,128)(2,1)} %get-tuple-element.9) | copy-start | bytes 18874372
  102.8 13.5 %copy-start.3 = (bf16[768,192]{0,1:T(8,128)(2,1)S(1)}, bf16[768,192]{0,1:T(8,128)(2,1)}, u32[]{:S(2)}) copy-start(bf16[768,192]{0,1:T(8,128)(2,1)} %param.23) | copy-start | bytes 884740
  102.8 13.8 %copy-start.4 = (bf16[768,192]{0,1:T(8,128)(2,1)S(1)}, bf16[768,192]{0,1:T(8,128)(2,1)}, u32[]{:S(2)}) copy-start(bf16[768,192]{0,1:T(8,128)(2,1)} %param.22) | copy-start | bytes 884740
  102.8 16.9 %copy-start.8 = (f32[12]{0:T(128)S(1)}, f32[12]{0:T(128)}, u32[]{:S(2)}) copy-start(f32[12]{0:T(128)} %param.21) | copy-start | bytes 148
  111.8 8.5 %copy-start.2 = (bf16[1024,896]{1,0:T(8,128)(2,1)}, bf16[1024,896]{1,0:T(8,128)(2,1)S(1)}, u32[]{:S(2)}) copy-start(bf16[1024,896]{1,0:T(8,128)(2,1)S(1)} %fusion.7.proj_ref) | copy-start | bytes 5505028
  111.9 8.4 %collective-permute-start = (bf16[2,192]{1,0:T(2,128)(2,1)S(1)}, bf16[2,192]{1,0:T(2,128)(2,1)S(1)}, u32[]{:S(2)}, u32[]{:S(2)}) collective-permute-start(bf16[2,192]{1,0:T(2,128)(2,1)S(1)} %fusion.10), channel_id=1, source_target_pairs={{0,8},{2,10},{4,12},{6,14},{8,16},{10,18},{12,20},{14,22},{16,24},... | collective-permute-start | bytes 2312 | tf_op jit(solution)/shard_map/ppermute | solution.py:22
  113.2 7.1 %collective-permute-start.1 = (bf16[128,128]{1,0:T(8,128)(2,1)S(1)}, bf16[128,128]{1,0:T(8,128)(2,1)S(1)}, u32[]{:S(2)}, u32[]{:S(2)}) collective-permute-start(bf16[128,128]{1,0:T(8,128)(2,1)S(1)} %slice.19), channel_id=1, source_target_pairs={{0,8},{2,10},{4,12},{6,14},{8,16},{10,18},{12,20},{14,22},{16,24},... | collective-permute-start | bytes 98312 | tf_op jit(solution)/shard_map/ppermute | solution.py:22
  120.3 0.6 copy-start.6
  120.3 0.6 copy-start.5

commit v3 on v2

--- a/solution.py
+++ b/solution.py
@@ -179,7 +179,7 @@
     pl.semaphore_wait(barrier, PLANE + beside)
 
 
-def gather_in_kernel(count, tok_ref, w_ref, x_ref, wg_ref, lsem, ws, wr, ts, tr, ds, dr, us, ur, vs, vr):
+def gather_in_kernel(count, tok_ref, w_ref, gain_ref, out_ref, x_ref, wg_ref, nrm_ref, acc_ref, ws, wr, ts, tr, ds, dr, us, ur, vs, vr):
     me, core, layer, spot, layers = place(count)
     rows, half = tok_ref.shape
     partner = {"sp": me, "tp": 1 - core}
@@ -194,7 +194,7 @@
         return lax.rem(spot + PLANE - k, PLANE)
 
     def x_slot(p):
-        return x_ref.at[pl.ds(pl.multiple_of(p * rows, rows), rows), pl.ds(pl.multiple_of(core * half, half), half)]
+        return x_ref.at[core, pl.ds(pl.multiple_of(p * rows, rows), rows)]
 
     def z_copy(up, d, k, own):
         p = source(k)
@@ -243,12 +243,8 @@
         for k in range(1, PLANE)
     ]
     d_copies = [start_to(tok_ref, x_slot(spot), ds.at[0], dr.at[0], partner)]
-    local = [
-        pltpu.make_async_copy(tok_ref, x_slot(spot), lsem.at[0]),
-        pltpu.make_async_copy(w_ref.at[spot], wg_ref.at[layer, spot], lsem.at[1]),
-    ]
-    for copy in local:
-        copy.start()
+    x_ref[core, pl.ds(pl.multiple_of(spot * rows, rows), rows), :] = tok_ref[...]
+    wg_ref[layer, spot] = w_ref[spot]
     for k in range(1, PLANE):
         pltpu.make_async_remote_copy(
             src_ref=w_ref.at[spot], dst_ref=wg_ref.at[layer, source(k)], send_sem=ws.at[k], recv_sem=wr.at[k],
@@ -285,26 +281,67 @@
             device_id=partner, device_id_type=MESH,
         ).wait_recv()
         d_copies.append(start_to(x_slot(p), x_slot(p), ds.at[k], dr.at[k], partner))
-    for d in range(2, layers):
-        receive_layer(d)
-    for copy in w_copies + t_copies:
-        copy.wait_send()
-    for k, copy in enumerate(d_copies):
-        copy.wait_send()
-        p = source(k)
+    for k in range(PLANE):
         pltpu.make_async_remote_copy(
             src_ref=tok_ref,
-            dst_ref=x_ref.at[pl.ds(pl.multiple_of(p * rows, rows), rows), pl.ds(pl.multiple_of((1 - core) * half, half), half)],
+            dst_ref=x_ref.at[1 - core, pl.ds(pl.multiple_of(source(k) * rows, rows), rows)],
             send_sem=ds.at[k], recv_sem=dr.at[k], device_id=partner, device_id_type=MESH,
         ).wait_recv()
+    length = PLANE * rows
+    span = 2 * half // layers
+    strip, tall = 32, 256
+
+    def normalise(i, carry):
+        at = pl.ds(pl.multiple_of(i * strip, strip), strip)
+        whole = jnp.concatenate([x_ref[0, at, :], x_ref[1, at, :]], axis=1).astype(jnp.float32)
+        mean = jnp.sum(whole * whole, axis=1, keepdims=True) / (2 * half)
+        scaled = (whole * lax.rsqrt(mean + 1e-06) * gain_ref[...]).astype(jnp.bfloat16)
+        for j in range(layers):
+            nrm_ref[j, at, :] = scaled[:, j * span : (j + 1) * span]
+        return carry
+
+    lax.fori_loop(0, length // strip, normalise, 0)
+
+    def add_layer(origin, fresh):
+        def step(i, carry):
+            at = pl.ds(pl.multiple_of(i * tall, tall), tall)
+            product = jnp.dot(
+                nrm_ref[origin, at, :],
+                wg_ref[origin].reshape(span, wg_ref.shape[3]),
+                preferred_element_type=jnp.float32,
+            )
+            acc_ref[at, :] = product if fresh else acc_ref[at, :] + product
+            return carry
+
+        lax.fori_loop(0, length // tall, step, 0)
+
+    def add_both(d):
+        @pl.when(layer >= d)
+        def _():
+            add_layer(layer - d, False)
+
+        @pl.when(layer + d < layers)
+        def _():
+            add_layer(layer + d, False)
+
+    for d in range(2, layers - 1):
+        receive_layer(d)
+    add_layer(layer, True)
+    for d in range(1, layers - 1):
+        add_both(d)
+    if layers > 2:
+        receive_layer(layers - 1)
+    if layers > 1:
+        add_both(layers - 1)
+    out_ref[...] = acc_ref[...].astype(out_ref.dtype)
+    for copy in w_copies + t_copies + d_copies:
+        copy.wait_send()
     for d in range(layers - 1):
         for k in range(PLANE):
             both(d, k, d == 0 and k == 0, "wait_send")
-    for copy in local:
-        copy.wait()
-
-
-def gather_in(count, tokens, wblocks):
+
+
+def gather_in(count, tokens, wblocks, gain):
     layers = count // PLANE
     rows, half = tokens.shape
     _, depth, cols = wblocks.shape
@@ -312,15 +349,21 @@
     hops = max(layers - 1, 1)
     return pl.pallas_call(
         functools.partial(gather_in_kernel, count),
-        out_shape=(
-            jax.ShapeDtypeStruct((PLANE * rows, 2 * half), tokens.dtype),
-            jax.ShapeDtypeStruct((layers, PLANE, depth, cols), wblocks.dtype),
+        out_shape=jax.ShapeDtypeStruct((PLANE * rows, cols), jnp.bfloat16),
+        in_specs=[pl.BlockSpec(memory_space=pltpu.VMEM)] * 3,
+        out_specs=pl.BlockSpec(memory_space=pltpu.VMEM),
+        scratch_shapes=[
+            pltpu.VMEM((2, PLANE * rows, half), tokens.dtype),
+            pltpu.VMEM((layers, PLANE, depth, cols), wblocks.dtype),
+            pltpu.VMEM((layers, PLANE * rows, 2 * half // layers), jnp.bfloat16),
+            pltpu.VMEM((PLANE * rows, cols), jnp.float32),
+        ]
+        + [dma((PLANE,))] * 6
+        + [dma((hops, PLANE))] * 4,
+        compiler_params=pltpu.CompilerParams(
+            collective_id=0, has_side_effects=True, vmem_limit_bytes=48 << 20
         ),
-        in_specs=[pl.BlockSpec(memory_space=pltpu.VMEM)] * 2,
-        out_specs=[pl.BlockSpec(memory_space=pl.ANY)] * 2,
-        scratch_shapes=[dma((2,))] + [dma((PLANE,))] * 6 + [dma((hops, PLANE))] * 4,
-        compiler_params=pltpu.CompilerParams(collective_id=0, has_side_effects=True),
-    )(tokens, wblocks)
+    )(tokens, wblocks, gain)
 
 
 def gather_out_kernel(count, h_ref, o_ref, hg_ref, og_ref, held, lsem, ts, tr, ds, dr, us, ur, vs, vr, es, er, fs):
@@ -474,7 +517,7 @@
     )(hidden, out_t)
 
 
-def exchange_kernel(y_ref, out_ref, lsem, ss, rs):
+def exchange_kernel(h_ref, o_ref, out_ref, y_ref, ss, rs):
     me, core = lax.axis_index("sp"), lax.axis_index("tp")
     spot = lax.rem(me, PLANE)
     first = me - spot
@@ -489,31 +532,46 @@
     for k in range(1, group):
         pl.semaphore_signal(barrier, inc=1, device_id=target(k)[1], device_id_type=MESH)
     pl.semaphore_wait(barrier, group - 1)
+    rows = out_ref.shape[1]
+
+    def product(other):
+        at = pl.ds(pl.multiple_of(other * rows, rows), rows)
+        return lax.dot_general(
+            h_ref[at, :], o_ref[...], (((1,), (1,)), ((), ())), preferred_element_type=jnp.float32
+        ).astype(out_ref.dtype)
+
     copies = []
+
+    def send(k):
+        copies.append(start_to(y_ref.at[k], out_ref.at[mine], ss.at[k], rs.at[k], target(k)[1]))
+
     for k in range(1, group):
-        other, device = target(k)
-        copies.append(start_to(y_ref.at[other], out_ref.at[mine], ss.at[k], rs.at[k], device))
-    local = pltpu.make_async_copy(y_ref.at[mine], out_ref.at[mine], lsem.at[0])
-    local.start()
+        y_ref[k] = product(target(k)[0])
+        if k > 1:
+            send(k - 1)
+    out_ref[mine] = product(mine)
+    send(group - 1)
     for k in range(1, group):
         copies[k - 1].wait_send()
         pltpu.make_async_remote_copy(
-            src_ref=y_ref.at[mine], dst_ref=out_ref.at[lax.rem(mine + group - k, group)], send_sem=ss.at[k],
+            src_ref=y_ref.at[0], dst_ref=out_ref.at[lax.rem(mine + group - k, group)], send_sem=ss.at[k],
             recv_sem=rs.at[k], device_id=target(k)[1], device_id_type=MESH,
         ).wait_recv()
-    local.wait()
-
-
-def exchange(blocks):
+
+
+def exchange(hidden, out_t):
     dma = pltpu.SemaphoreType.DMA
+    blocks = (2 * PLANE, hidden.shape[0] // (2 * PLANE), out_t.shape[0])
     return pl.pallas_call(
         exchange_kernel,
-        out_shape=jax.ShapeDtypeStruct(blocks.shape, blocks.dtype),
-        in_specs=[pl.BlockSpec(memory_space=pltpu.VMEM)],
+        out_shape=jax.ShapeDtypeStruct(blocks, hidden.dtype),
+        in_specs=[pl.BlockSpec(memory_space=pltpu.VMEM)] * 2,
         out_specs=pl.BlockSpec(memory_space=pltpu.VMEM),
-        scratch_shapes=[dma((1,)), dma((2 * PLANE,)), dma((2 * PLANE,))],
-        compiler_params=pltpu.CompilerParams(collective_id=2, has_side_effects=True),
-    )(blocks)
+        scratch_shapes=[pltpu.VMEM(blocks, hidden.dtype), dma((2 * PLANE,)), dma((2 * PLANE,))],
+        compiler_params=pltpu.CompilerParams(
+            collective_id=2, has_side_effects=True, vmem_limit_bytes=40 << 20
+        ),
+    )(hidden, out_t)
 
 
 def pack_kernel(*refs):
@@ -629,12 +687,7 @@
     group = QHEADS // KVHEADS
 
     wblocks = pack((outer_gate_w, inner_gate_w, signal_w, query_w, key_w, value_w))
-    x, weights = gather_in(count, tokens, wblocks)
-    x32 = x.astype(f32)
-    normed = (
-        x32 * lax.rsqrt(jnp.mean(x32 * x32, axis=-1, keepdims=True) + 1e-06) * norm_gain
-    ).astype(bf16)
-    proj = jnp.dot(normed, weights.reshape(x.shape[1], -1), preferred_element_type=f32).astype(bf16)
+    proj = gather_in(count, tokens, wblocks, norm_gain.reshape(1, -1))
     length = proj.shape[0]
     last = proj[length - TAPS + 1 :, chans : 3 * chans].astype(f32)
     before = from_behind((last[:, :chans] * last[:, chans:]).astype(bf16), "sp", PLANE)
@@ -649,10 +702,7 @@
         [out_conv_w.reshape(PLANE, chans, cols), out_attn_w.reshape(PLANE, wide, cols)], axis=1
     ).reshape(-1, cols).T
     hidden_all, out_all = gather_out(count, hidden, out_t)
-    result = lax.dot_general(
-        hidden_all, out_all, (((1,), (1,)), ((), ())), preferred_element_type=f32
-    ).astype(bf16)
-    swapped = exchange(result.reshape(2 * PLANE, length // (2 * PLANE), -1))
+    swapped = exchange(hidden_all, out_all)
     rows = length // (2 * PLANE)
     swapped = swapped.reshape(PLANE, 2, rows, layers, cols // 2).transpose(2, 3, 0, 1, 4)
     return swapped.reshape(rows, -1)

time: 209 us -> 193 us (0.923)
  matrix products: 16.7 us -> 0 us
  local copies, waits for them, and re-layouts: 6.67 us -> 11.6 us
  other arithmetic: 5.41 us -> 1.92 us
    dot_general x2 -> x0, matrix products: 16.7 us -> none  [the longest x1 8.95 us: plane_body(): jnp.dot(normed, weights.reshape(x.shape[1], -1), preferred_element_type=f32)]
    unnamed x19 -> x25, local copies, waits for them, and re-layouts: 1.95 us -> 7.39 us
    reduce_sum x1 -> x0, other arithmetic: 4.23 us -> none  [plane_body(): jnp.mean(x32 * x32, axis=-1, keepdims=True) + 1e-06]
where the time goes in v3:
time: 193 us
  Pallas kernels  177 us (92%)
  local copies, waits for them, and re-layouts  11.6 us (6%)
  starting transfers between devices  2.56 us (1%)
    pallas_call x1, Pallas kernels, gather_in(): pl.pallas_call(functools.partial(gather_in_kernel, count), out_shape=jax....  96.3 us
    pallas_call x1, Pallas kernels, gather_out(): pl.pallas_call(functools.partial(gather_out_kernel, count), out_shape=(ja...  49.8 us
    pallas_call x1, Pallas kernels, exchange(): pl.pallas_call(exchange_kernel, out_shape=jax.ShapeDtypeStruct(blocks, hi...  17.2 us
    pallas_call x1, Pallas kernels, mixer(): pl.pallas_call(functools.partial(mixer_kernel, chans, wide), out_shape=ja...  10.4 us
    unnamed x25, local copies, waits for them, and re-layouts  7.39 us
  transfers between devices with their start and end apart: 2, of which 0 were waited for; matrix products, arithmetic and copies ran while one was open for 2% of the time, Pallas kernels for 0%

profile of v3, /device:TPU:1, one launch (start us, length us, event | category | flops | bytes accessed | tf_op | source)
XLA Modules:
  0.0 192.9 jit_solution(9542996347511746867)
XLA Ops:
  0.0 0.0 copy-start
  0.0 2.8 %shard_map.118.w_ref = bf16[4,192,896]{2,1,0:T(8,128)(2,1)} custom-call(bf16[192,768]{1,0:T(8,128)(2,1)} %refs_0_.1, bf16[192,768]{1,0:T(8,128)(2,1)} %refs_1_.1, bf16[192,768]{1,0:T(8,128)(2,1)} %refs_2_.1, bf16[192,768]{1,0:T(8,128)(2,1)} %refs_3_.1, bf16[192,256]{1,0:T(8,128)(2,1)} %refs_4_.1, bf16[192,256]{1,0:T(8,128)(2,1)} %refs_5_.1), custom_call_target="tpu_custom_call" | custom-call | tf_op jit(solution)/shard_map/pallas_call | solution.py:590
  2.8 0.0 copy-done.6
  2.8 1.3 copy-done.3
  4.1 96.3 %shard_map.119.proj_ref = bf16[1024,896]{1,0:T(8,128)(2,1)S(1)} custom-call(bf16[256,1536]{1,0:T(8,128)(2,1)S(1)} %copy-done.5, bf16[4,192,896]{2,1,0:T(8,128)(2,1)S(1)} %copy-done.3, f32[1,3072]{1,0:T(1,128)S(1)} %bitcast.16), custom_call_target="tpu_custom_call" | custom-call | tf_op jit(solution)/shard_map/pallas_call | solution.py:350
  100.5 0.1 slice_convert_fusion
  100.5 0.9 fusion
  101.4 1.3 collective-permute-start
  102.7 0.6 slice.15
  103.3 1.3 collective-permute-start.1
  104.6 0.0 copy-start.11
  104.6 0.4 reshape.23
  105.0 0.4 reshape.24
  105.4 0.0 copy-done
  105.4 0.7 constant_dynamic-slice_fusion.taps_ref
  106.1 0.5 pad_maximum_fusion
  106.6 0.5 multiply_exponential_fusion.slopes_ref
  107.0 1.0 copy.17
  108.0 0.0 copy-done.1
  108.0 0.6 dynamic_slice.6.sinks_ref
  108.7 0.0 collective-permute-done.before_ref
  108.7 0.0 collective-permute-done.1.kv_before_ref
  108.7 0.6 copy-done.10
  109.3 0.0 copy-done.9
  109.3 10.4 %shard_map.120.h_ref = bf16[1024,384]{1,0:T(8,128)(2,1)} custom-call(f32[3]{0:T(128)} %multiply_exponential_fusion.slopes_ref, f32[3]{0:T(128)} %dynamic_slice.6.sinks_ref, s32[1]{0:T(128)} %bitcast.offset_ref, bf16[1024,896]{1,0:T(8,128)(2,1)} %copy-done.1, bf16[2,192]{1,0:T(2,128)(2,1)} %copy-done.10, bf16[128,128]{1,0:T(8,128)(2,1)} %copy-done.9, ...), custom_call_target="tpu_custom_call" | custom-call | tf_op jit(solution)/shard_map/pallas_call | solution.py:653
  119.7 49.8 %shard_map.121 = (bf16[1024,3072]{1,0:T(8,128)(2,1)}, bf16[384,3072]{1,0:T(8,128)(2,1)}) custom-call(bf16[1024,384]{1,0:T(8,128)(2,1)} %shard_map.120.h_ref, bf16[192,1536]{1,0:T(8,128)(2,1)} %bitcast.19), custom_call_target="tpu_custom_call" | custom-call | tf_op jit(solution)/shard_map/pallas_call | solution.py:504
  169.6 2.8 %copy-done.2 = bf16[1024,3072]{1,0:T(8,128)(2,1)S(1)} copy-done((bf16[1024,3072]{1,0:T(8,128)(2,1)S(1)}, bf16[1024,3072]{1,0:T(8,128)(2,1)}, u32[]{:S(2)}) %copy-start.2) | copy-done | bytes 6291480
  172.3 1.7 copy-done.4
  174.0 17.2 %shard_map.122 = bf16[8,128,384]{2,1,0:T(8,128)(2,1)S(1)} custom-call(bf16[1024,3072]{1,0:T(8,128)(2,1)S(1)} %copy-done.2, bf16[384,3072]{1,0:T(8,128)(2,1)S(1)} %copy-done.4), custom_call_target="tpu_custom_call" | custom-call | tf_op jit(solution)/shard_map/pallas_call | solution.py:565
  191.2 0.4 copy.14
  191.6 0.1 copy.15
  191.7 1.2 copy.16
  (14 shorter events, 0.0 us)
Async XLA Ops:
  0.0 105.4 %copy-start = (f32[3,768]{1,0:T(4,128)S(1)}, f32[3,768]{1,0:T(4,128)}, u32[]{:S(2)}) copy-start(f32[3,768]{1,0:T(4,128)} %param.17) | copy-start | bytes 27652
  0.0 2.8 %copy-start.6 = (f32[3072]{0:T(1024)S(1)}, f32[3072]{0:T(1024)}, u32[]{:S(2)}) copy-start(f32[3072]{0:T(1024)} %param.13) | copy-start | bytes 36868
  0.0 2.8 %copy-start.5 = (bf16[256,1536]{1,0:T(8,128)(2,1)S(1)}, bf16[256,1536]{1,0:T(8,128)(2,1)}, u32[]{:S(2)}) copy-start(bf16[256,1536]{1,0:T(8,128)(2,1)} %tok_ref.1) | copy-start | bytes 2359300
  2.8 1.3 copy-start.3
  4.1 100.5 %copy-start.7 = (bf16[768,192]{0,1:T(8,128)(2,1)S(1)}, bf16[768,192]{0,1:T(8,128)(2,1)}, u32[]{:S(2)}) copy-start(bf16[768,192]{0,1:T(8,128)(2,1)} %param.22) | copy-start | bytes 884740
  4.1 100.9 %copy-start.8 = (bf16[768,192]{0,1:T(8,128)(2,1)S(1)}, bf16[768,192]{0,1:T(8,128)(2,1)}, u32[]{:S(2)}) copy-start(bf16[768,192]{0,1:T(8,128)(2,1)} %param.23) | copy-start | bytes 884740
  100.5 7.6 %copy-start.1 = (bf16[1024,896]{1,0:T(8,128)(2,1)}, bf16[1024,896]{1,0:T(8,128)(2,1)S(1)}, u32[]{:S(2)}) copy-start(bf16[1024,896]{1,0:T(8,128)(2,1)S(1)} %shard_map.119.proj_ref) | copy-start | bytes 5505028
  101.4 7.3 %collective-permute-start = (bf16[2,192]{1,0:T(2,128)(2,1)}, bf16[2,192]{1,0:T(2,128)(2,1)S(1)}, u32[]{:S(2)}, u32[]{:S(2)}) collective-permute-start(bf16[2,192]{1,0:T(2,128)(2,1)} %fusion), channel_id=1, source_target_pairs={{0,8},{2,10},{4,12},{6,14},{8,16},{10,18},{12,20},{14,22},{16,24},... | collective-permute-start | bytes 2312 | tf_op jit(solution)/shard_map/ppermute | solution.py:22
  103.3 5.4 %collective-permute-start.1 = (bf16[128,128]{1,0:T(8,128)(2,1)}, bf16[128,128]{1,0:T(8,128)(2,1)S(1)}, u32[]{:S(2)}, u32[]{:S(2)}) collective-permute-start(bf16[128,128]{1,0:T(8,128)(2,1)} %slice.15), channel_id=1, source_target_pairs={{0,8},{2,10},{4,12},{6,14},{8,16},{10,18},{12,20},{14,22},{16,24},... | collective-permute-start | bytes 98312 | tf_op jit(solution)/shard_map/ppermute | solution.py:22
  104.6 3.4 %copy-start.11 = (f32[12]{0:T(128)S(1)}, f32[12]{0:T(128)}, u32[]{:S(2)}) copy-start(f32[12]{0:T(128)} %param.21) | copy-start | bytes 148
  108.7 0.6 copy-start.10
  108.7 0.6 copy-start.9
  169.6 2.8 %copy-start.2 = (bf16[1024,3072]{1,0:T(8,128)(2,1)S(1)}, bf16[1024,3072]{1,0:T(8,128)(2,1)}, u32[]{:S(2)}) copy-start(bf16[1024,3072]{1,0:T(8,128)(2,1)} %get-tuple-element.7.h_ref) | copy-start | bytes 18874372
  172.3 1.7 copy-start.4
